TPU v7x, 32 devices: a whole 2x2x4 slice. The times are simulated.
32 devices in a mesh: sp: 8 (over z, x), tp: 4 (over y, core).
Axes of the slice: x: 2, y: 2, z: 4, core: 2. Of those that a mesh axis runs over, the one named last changes fastest.
Arguments:
- glu_a: bfloat16 [2048, 1024], P('sp', 'tp'), may hold values from -6 to 6
- glu_b: bfloat16 [2048, 1024], P('sp', 'tp'), may hold values from -6 to 6
- saved_conv: bfloat16 [2048, 1024], P('sp', 'tp')
- taps: float32 [31, 1024], P(None, 'tp'), may hold values from -1 to 1
- norm_gain_vector: float32 [1024], P('tp'), may hold values from 0.1 to 1.9
- out_proj: bfloat16 [1024, 2048], P('tp'), may hold values from -0.1875 to 0.1875
- moe_in: bfloat16 [2048, 2048], P('sp'), may hold values from -6 to 6
- grad_out: bfloat16 [2048, 2048], P('sp'), may hold values from -6 to 6
- expert_ids: int32 [2048, 2], P('sp'), may hold values from 0 to 7, all different within a row; in each aligned block of 256 rows (0 to 255, 256 to 511, ...) at most 96 rows name the same one
- route_weights: float32 [2048, 2], P('sp'), may hold values from 0.3 to 2
- w_gate: bfloat16 [8, 2048, 1024], P('sp', None, 'tp'), may hold values from -0.125 to 0.125
- w_up: bfloat16 [8, 2048, 1024], P('sp', None, 'tp'), may hold values from -0.125 to 0.125
- w_down: bfloat16 [8, 1024, 2048], P('sp', 'tp'), may hold values from -0.1875 to 0.1875
Outputs:
- grad_glu_a: bfloat16 [2048, 1024], P('sp', 'tp')
- grad_glu_b: bfloat16 [2048, 1024], P('sp', 'tp')
- grad_out_proj: float32 [2048, 1024], P('sp', 'tp')
- grad_gate: bfloat16 [8, 2048, 1024], P('sp', None, 'tp')
- grad_up: bfloat16 [8, 2048, 1024], P('sp', None, 'tp')
- grad_down: bfloat16 [8, 1024, 2048], P('sp', 'tp')
Inputs may be any that keep to these rules, and one draw needn't show every extreme that they name: `expert_ids`: in each aligned block of 256 tokens, a token's 2 experts differ, and no expert is named more than 96 times; some expert reaches 96 in some blocks.
All inputs are finite; a program needn't handle non-finite values.
Results may differ from a plain program's by a relative error of at most 0.015.
Values may be sent and summed in bfloat16 or wider, within the bound.
A program may use at most 64 MiB of HBM per device.

v0:
```python
import jax
import jax.numpy as jnp
from jax import lax
from jax.sharding import PartitionSpec as P

CONV_CHANNELS = 1024


def with_halo(array, sides, width):
    for axis, dim in sides:
        size, length = (lax.axis_size(axis), array.shape[dim])
        up = [(i, (i + 1) % size) for i in range(size - 1)]
        down = [(j, i) for i, j in up]
        last = lax.slice_in_dim(array, length - width, length, axis=dim)
        initial = lax.slice_in_dim(array, 0, width, axis=dim)
        before = lax.ppermute(last, axis, up)
        after = lax.ppermute(initial, axis, down)
        array = jnp.concatenate([before, array, after], axis=dim)
    return array


def expert_local(in_rows, cot_rows, w_gate, w_up, w_down):
    gate_pre = jnp.einsum("esd,edf->esf", in_rows, w_gate, preferred_element_type=jnp.float32)
    up_pre = jnp.einsum("esd,edf->esf", in_rows, w_up, preferred_element_type=jnp.float32)
    sig_gate = jax.nn.sigmoid(gate_pre)
    act_gate = gate_pre * sig_gate
    hidden = (act_gate * up_pre).astype(jnp.bfloat16)
    grad_hidden = jnp.einsum("esd,efd->esf", cot_rows, w_down, preferred_element_type=jnp.float32)
    grad_upact = (grad_hidden * act_gate).astype(jnp.bfloat16)
    grad_gateact = (grad_hidden * up_pre * sig_gate * (1.0 + gate_pre * (1.0 - sig_gate))).astype(
        jnp.bfloat16
    )
    return (hidden, grad_upact, grad_gateact)


def weight_grads(in_rows, cot_rows, hidden, grad_upact, grad_gateact):
    grad_down = jnp.einsum(
        "esf,esd->efd", hidden, cot_rows, preferred_element_type=jnp.float32
    ).astype(jnp.bfloat16)
    grad_gate = jnp.einsum(
        "esd,esf->edf", in_rows, grad_gateact, preferred_element_type=jnp.float32
    ).astype(jnp.bfloat16)
    grad_up = jnp.einsum(
        "esd,esf->edf", in_rows, grad_upact, preferred_element_type=jnp.float32
    ).astype(jnp.bfloat16)
    return (grad_gate, grad_up, grad_down)


def per_device(
    glu_a,
    glu_b,
    saved_conv,
    taps,
    norm_gain_vector,
    out_proj,
    moe_in,
    grad_out,
    expert_ids,
    route_weights,
    w_gate,
    w_up,
    w_down,
):
    n_sp = lax.axis_size("sp")
    n_tp = lax.axis_size("tp")
    tp_pos = lax.axis_index("tp")
    tok_dev, d_model = grad_out.shape
    top_count = expert_ids.shape[1]
    exp_dev = w_gate.shape[0]
    experts = exp_dev * n_sp
    capacity = max(2, 3 * tok_dev * top_count // (2 * experts))
    quarter = d_model // n_tp
    pair_count = tok_dev * top_count
    flat_ids = expert_ids.reshape(pair_count)
    onehot = (flat_ids[:, None] == jnp.arange(experts, dtype=jnp.int32)[None, :]).astype(jnp.int32)
    slot_rank = jnp.sum((jnp.cumsum(onehot, axis=0) - onehot) * onehot, axis=1)
    slot_of = flat_ids * capacity + slot_rank
    owner_idx = (
        jnp.full((experts * capacity,), pair_count, jnp.int32)
        .at[slot_of]
        .set(jnp.arange(pair_count, dtype=jnp.int32))
    )
    token_idx = owner_idx // top_count
    scaled = (grad_out.astype(jnp.float32)[:, None, :] * route_weights[:, :, None]).astype(
        jnp.bfloat16
    )
    scaled = scaled.reshape(pair_count, d_model)

    def to_expert(rows):
        width = rows.shape[1]
        return (
            rows.reshape(n_sp, exp_dev, capacity, width)
            .swapaxes(0, 1)
            .reshape(exp_dev, n_sp * capacity, width)
        )

    in_part = lax.dynamic_slice_in_dim(moe_in, tp_pos * quarter, quarter, 1)
    cot_part = lax.dynamic_slice_in_dim(scaled, tp_pos * quarter, quarter, 1)
    in_pad = jnp.concatenate([in_part, jnp.zeros((1, quarter), jnp.bfloat16)], axis=0)
    cot_pad = jnp.concatenate([cot_part, jnp.zeros((1, quarter), jnp.bfloat16)], axis=0)
    sent_in, sent_cot = (
        lax.all_to_all(in_pad[token_idx], "sp", split_axis=0, concat_axis=0, tiled=True),
        lax.all_to_all(cot_pad[owner_idx], "sp", split_axis=0, concat_axis=0, tiled=True),
    )
    recv_in, recv_cot = (
        lax.all_gather(sent_in, "tp", axis=1, tiled=True),
        lax.all_gather(sent_cot, "tp", axis=1, tiled=True),
    )
    in_rows = to_expert(recv_in)
    cot_rows = to_expert(recv_cot)
    hidden, grad_upact, grad_gateact = expert_local(in_rows, cot_rows, w_gate, w_up, w_down)
    grad_gate, grad_up, grad_down = weight_grads(
        in_rows, cot_rows, hidden, grad_upact, grad_gateact
    )
    partial_value = jnp.einsum(
        "esf,edf->esd", grad_gateact, w_gate, preferred_element_type=jnp.float32
    )
    partial_value = partial_value + jnp.einsum(
        "esf,edf->esd", grad_upact, w_up, preferred_element_type=jnp.float32
    )
    partial_value = partial_value.astype(jnp.bfloat16)
    row_grads = (
        lax.psum_scatter(partial_value, "tp", scatter_dimension=2, tiled=True)
        .astype(jnp.float32)
        .astype(jnp.bfloat16)
    )
    row_grads = (
        row_grads.reshape(exp_dev, n_sp, capacity, quarter)
        .swapaxes(0, 1)
        .reshape(n_sp * exp_dev * capacity, quarter)
    )
    returned = lax.all_to_all(row_grads, "sp", split_axis=0, concat_axis=0, tiled=True)
    picked = returned[slot_of].reshape(tok_dev, top_count, quarter).astype(jnp.float32)
    grad_own = lax.dynamic_slice_in_dim(grad_out, tp_pos * quarter, quarter, 1).astype(jnp.float32)
    mix_part = (grad_own + jnp.sum(picked, axis=1)).astype(jnp.bfloat16)
    grad_mix = lax.all_gather(mix_part, "tp", axis=1, tiled=True)
    head_gradient = lax.dot_general(
        grad_mix, out_proj, (((1,), (1,)), ((), ())), preferred_element_type=jnp.float32
    )
    convolved_rows = saved_conv.astype(jnp.float32)
    sum_c, sum_sq = lax.psum(
        (jnp.sum(convolved_rows, axis=1), jnp.sum(convolved_rows * convolved_rows, axis=1)), "tp"
    )
    channel_average = (sum_c / CONV_CHANNELS)[:, None]
    var_c = (sum_sq / CONV_CHANNELS)[:, None] - channel_average * channel_average
    inverse_deviation = lax.rsqrt(var_c + 1e-05)
    centered_scaled = (convolved_rows - channel_average) * inverse_deviation
    normalized_rows = centered_scaled * norm_gain_vector[None, :]
    sigmoid_of_norm = jax.nn.sigmoid(normalized_rows)
    heads = (normalized_rows * sigmoid_of_norm).astype(jnp.bfloat16)
    grad_out_proj = lax.psum_scatter(
        lax.dot_general(
            grad_mix, heads, (((0,), (0,)), ((), ())), preferred_element_type=jnp.float32
        ),
        "sp",
        scatter_dimension=0,
        tiled=True,
    )
    normalized_gradient = (
        head_gradient
        * sigmoid_of_norm
        * (1.0 + normalized_rows * (1.0 - sigmoid_of_norm))
        * norm_gain_vector[None, :]
    )
    gradient_total, product_total = lax.psum(
        (
            jnp.sum(normalized_gradient, axis=1),
            jnp.sum(normalized_gradient * centered_scaled, axis=1),
        ),
        "tp",
    )
    convolved_gradient = (
        inverse_deviation
        * (
            normalized_gradient
            - (gradient_total / CONV_CHANNELS)[:, None]
            - centered_scaled * (product_total / CONV_CHANNELS)[:, None]
        )
    ).astype(jnp.bfloat16)
    reach = (taps.shape[0] - 1) // 2
    padded = with_halo(convolved_gradient, (("sp", 0),), reach).astype(jnp.float32)
    grad_y = jnp.zeros(head_gradient.shape, jnp.float32)
    for tap_idx in range(taps.shape[0]):
        grad_y = (
            grad_y
            + taps[tap_idx][None, :] * padded[2 * reach - tap_idx : 2 * reach - tap_idx + tok_dev]
        )
    sig_b = jax.nn.sigmoid(glu_b.astype(jnp.float32))
    grad_glu_a = (grad_y * sig_b).astype(jnp.bfloat16)
    grad_glu_b = (grad_y * glu_a.astype(jnp.float32) * sig_b * (1.0 - sig_b)).astype(jnp.bfloat16)
    return (grad_glu_a, grad_glu_b, grad_out_proj, grad_gate, grad_up, grad_down)


def solution(mesh):
    in_specs = (
        P("sp", "tp"),
        P("sp", "tp"),
        P("sp", "tp"),
        P(None, "tp"),
        P("tp"),
        P("tp", None),
        P("sp", None),
        P("sp", None),
        P("sp", None),
        P("sp", None),
        P("sp", None, "tp"),
        P("sp", None, "tp"),
        P("sp", "tp", None),
    )
    out_specs = (
        P("sp", "tp"),
        P("sp", "tp"),
        P("sp", "tp"),
        P("sp", None, "tp"),
        P("sp", None, "tp"),
        P("sp", "tp", None),
    )
    return jax.shard_map(
        per_device, mesh=mesh, in_specs=in_specs, out_specs=out_specs, check_vma=False
    )
```

profile of v0, /device:TPU:0, one launch (start us, length us, event | category | flops | bytes accessed | tf_op | source)
XLA Modules:
  0.0 280.5 jit_solution(9579719425612122031)
XLA Ops:
  9.4 1.1 reduce-window.6
  10.9 2.4 scatter_custom_fusion
  14.4 2.7 gather_fusion.1
  17.1 27.3 %all_to_all.36 = bf16[8,96,512]{2,1,0:T(8,128)(2,1)} all-to-all(bf16[8,96,512]{2,1,0:T(8,128)(2,1)S(1)} %bitcast.85), channel_id=1, replica_groups=mesh['sp'=8,'tp'=4] {'sp'}, dimensions={0} | all-to-all | bytes 1572864 | tf_op jit(solution)/shard_map/all_to_all | solution.py:102
  44.8 4.1 %mul.456 = f32[256,2,2048]{2,1,0:T(2,128)} broadcast(bf16[256,2048]{1,0:T(8,128)(2,1)S(1)} %copy-done.1), dimensions={0,2} | broadcast | bytes 5242880 | tf_op jit(solution)/shard_map/mul | solution.py:84
  48.9 6.4 %mul.457 = f32[512,2048]{1,0:T(8,128)} reshape(f32[256,2,2048]{2,1,0:T(2,128)} %mul.456) | data formatting | bytes 8388608 | tf_op jit(solution)/shard_map/mul | solution.py:84
  55.3 1.4 fusion.6
  56.7 2.7 gather_fusion
  59.4 23.1 %all_to_all.37 = bf16[8,96,512]{2,1,0:T(8,128)(2,1)} all-to-all(bf16[8,96,512]{2,1,0:T(8,128)(2,1)S(1)} %bitcast.86), channel_id=1, replica_groups=mesh['sp'=8,'tp'=4] {'sp'}, dimensions={0} | all-to-all | bytes 1572864 | tf_op jit(solution)/shard_map/all_to_all | solution.py:103
  82.7 3.9 %fusion.9 = f32[768,256]{1,0:T(8,128)} fusion(bf16[768,2048]{1,0:T(8,128)(2,1)} %all-gather.6.cloned.1.call-done, bf16[1,2048,256]{2,1,0:T(8,128)(2,1)S(1)} %copy-done), kind=kOutput, calls=%fused_computation.19 | convolution fusion | flops 805306368 | bytes 4980736 | tf_op jit(solution)/shard_map/esd,edf->esf/dot_general | solution.py:23
  86.6 1.9 fusion.12
  88.5 21.8 %all-gather.4.cloned.1.call-done = bf16[768,2048]{1,0:T(8,128)(2,1)} async-done(((bf16[768,512]{1,0:T(8,128)(2,1)}), bf16[768,2048]{1,0:T(8,128)(2,1)}) %all-gather.4.cloned.1.call-update) | async-done | bytes 3145744 | tf_op jit(solution)/shard_map/all_gather | solution.py:107
  110.3 3.8 %multiply_convert_fusion.1 = (bf16[768,256]{1,0:T(8,128)(2,1)S(1)}, bf16[768,256]{1,0:T(8,128)(2,1)S(1)}) fusion(f32[768,256]{1,0:T(8,128)} %fusion.9, f32[768,256]{1,0:T(8,128)} %fusion.12, bf16[768,2048]{1,0:T(8,128)(2,1)} %all-gather.4.cloned.1.call-done, bf16[1,256,2048]{2,1,0:T(8,128)(2,1)} %param.25), kind=kOutput, calls=%fused_computation.27 | convolution fusion | flops 807862272 | bytes 6553600 | tf_op jit(solution)/shard_map/esd,efd->esf/dot_general | solution.py:28
  114.1 1.0 fusion.7
  115.1 2.7 fusion
  117.9 37.9 %reduce-scatter.3.cloned.1.call-done = bf16[1,768,512]{2,1,0:T(8,128)(2,1)} async-done(((bf16[1,768,2048]{2,1,0:T(8,128)(2,1)}), bf16[1,768,512]{2,1,0:T(8,128)(2,1)}) %reduce-scatter.3.cloned.1.call-update) | async-done | bytes 786448 | tf_op jit(solution)/shard_map/reduce_scatter | solution.py:123
  155.8 5.5 %all-to-all-start.2 = ((bf16[8,96,512]{2,1,0:T(8,128)(2,1)}), bf16[8,96,512]{2,1,0:T(8,128)(2,1)S(1)}, u32[]{:S(2)}, u32[]{:S(2)}) async-start(bf16[8,96,512]{2,1,0:T(8,128)(2,1)} %bitcast.89), calls=%async_computation.3 | async-start | bytes 1572864 | tf_op jit(solution)/shard_map/all_to_all | solution.py:132
  161.5 19.8 %all-to-all-done.2 = bf16[8,96,512]{2,1,0:T(8,128)(2,1)S(1)} async-done(((bf16[8,96,512]{2,1,0:T(8,128)(2,1)}), bf16[8,96,512]{2,1,0:T(8,128)(2,1)S(1)}, u32[]{:S(2)}, u32[]{:S(2)}) %all-to-all-start.2) | async-done | bytes 786464 | tf_op jit(solution)/shard_map/all_to_all | solution.py:132
  181.4 2.0 gather_fusion.2
  184.0 1.2 reduce_sum.60
  185.3 1.7 add_convert_fusion.1
  187.2 5.9 %all-reduce.3 = (f32[256]{0:T(256)S(1)}, f32[256]{0:T(256)S(1)}) all-reduce(f32[256]{0:T(256)S(1)} %get-tuple-element.9, f32[256]{0:T(256)S(1)} %get-tuple-element.8), channel_id=1, replica_groups=mesh['sp'=8,'tp'=4] {'tp'}, use_global_device_ids=true, to_apply=%region_3.4 | all-reduce | flops 512 | bytes 4096 | tf_op jit(solution)/shard_map/psum | solution.py:141
  193.2 8.7 %all-gather.8.cloned.1.call-done = bf16[256,2048]{1,0:T(8,128)(2,1)} async-done(((bf16[256,512]{1,0:T(8,128)(2,1)}), bf16[256,2048]{1,0:T(8,128)(2,1)}) %all-gather.8.cloned.1.call-update) | async-done | bytes 1048592 | tf_op jit(solution)/shard_map/all_gather | solution.py:136
  201.9 3.2 %fusion.65 = f32[2048,256]{1,0:T(8,128)} fusion(bf16[256,2048]{1,0:T(8,128)(2,1)} %all-gather.8.cloned.1.call-done, bf16[256,256]{1,0:T(8,128)(2,1)S(1)} %copy-done.2, f32[256]{0:T(256)S(1)} %copy-done.9, f32[256]{0:T(256)S(1)} %get-tuple-element.54, f32[256]{0:T(256)S(1)} %get-tuple-element.53), kind=kOutput, calls=%fused_computation.117 | convolution fusion | flops 269025280 | bytes 3279872 | tf_op jit(solution)/shard_map/dot_general | solution.py:152
  205.1 4.0 %fusion.2 = bf16[1,2048,256]{2,1,0:T(8,128)(2,1)} fusion(bf16[768,2048]{1,0:T(8,128)(2,1)} %all-gather.6.cloned.1.call-done, bf16[768,256]{1,0:T(8,128)(2,1)S(1)} %get-tuple-element.16), kind=kOutput, calls=%fused_computation.10 | convolution fusion | flops 805830656 | bytes 4587520 | tf_op jit(solution)/shard_map/esd,esf->edf/dot_general | solution.py:43
  209.2 2.0 fusion.3
  211.8 6.3 %all-reduce.2 = (f32[256]{0:T(256)S(1)}, f32[256]{0:T(256)S(1)}) all-reduce(f32[256]{0:T(256)S(1)} %get-tuple-element.7, f32[256]{0:T(256)S(1)} %get-tuple-element.6), channel_id=1, replica_groups=mesh['sp'=8,'tp'=4] {'tp'}, use_global_device_ids=true, to_apply=%region_13.14 | all-reduce | flops 512 | bytes 4096 | tf_op jit(solution)/shard_map/psum | solution.py:165
  218.4 3.5 %collective-permute-start = (bf16[15,256]{1,0:T(8,128)(2,1)S(1)}, bf16[15,256]{1,0:T(8,128)(2,1)S(1)}, u32[]{:S(2)}, u32[]{:S(2)}) collective-permute-start(bf16[15,256]{1,0:T(8,128)(2,1)S(1)} %get-tuple-element.18), channel_id=1, source_target_pairs={{0,4},{4,8},{8,12},{12,16},{16,20},{20,24},{24,28},{1,5},{5,9},{9,... | collective-permute-start | bytes 23048 | tf_op jit(solution)/shard_map/ppermute | solution.py:16
  221.9 1.4 collective-permute-start.1
  223.4 3.9 %fusion.1 = bf16[1,2048,256]{2,1,0:T(8,128)(2,1)} fusion(bf16[768,2048]{1,0:T(8,128)(2,1)} %all-gather.6.cloned.1.call-done, bf16[768,256]{1,0:T(8,128)(2,1)S(1)} %get-tuple-element.17), kind=kOutput, calls=%fused_computation.9 | convolution fusion | flops 805830656 | bytes 4587520 | tf_op jit(solution)/shard_map/esd,esf->edf/dot_general | solution.py:40
  227.7 1.6 multiply_convert_fusion.4
  230.0 44.0 %reduce-scatter.5.cloned.1.call-done = f32[256,256]{1,0:T(8,128)} async-done(((f32[2048,256]{1,0:T(8,128)}), f32[256,256]{1,0:T(8,128)}) %reduce-scatter.5.cloned.1.call-update) | async-done | bytes 262160 | tf_op jit(solution)/shard_map/reduce_scatter | solution.py:151
  (76 shorter events, 7.2 us)
Async XLA Ops:
  7.2 75.5 %copy-start = (bf16[1,2048,256]{2,1,0:T(8,128)(2,1)S(1)}, bf16[1,2048,256]{2,1,0:T(8,128)(2,1)}, u32[]{:S(2)}) copy-start(bf16[1,2048,256]{2,1,0:T(8,128)(2,1)} %param.23) | copy-start | bytes 3145732
  7.2 75.5 %all-gather.6.cloned.1.call-start = ((), (), s32[]{:S(2)}) async-start(), calls=%async_computation.6 | async-start | bytes 3932160 | tf_op jit(solution)/shard_map/all_gather | solution.py:106
  14.4 30.1 %copy-start.8 = (f32[256,2]{0,1:T(2,128)S(1)}, f32[256,2]{0,1:T(2,128)}, u32[]{:S(2)}) copy-start(f32[256,2]{0,1:T(2,128)} %param.22) | copy-start | bytes 6148
  14.4 30.4 %copy-start.1 = (bf16[256,2048]{1,0:T(8,128)(2,1)S(1)}, bf16[256,2048]{1,0:T(8,128)(2,1)}, u32[]{:S(2)}) copy-start(bf16[256,2048]{1,0:T(8,128)(2,1)} %param.20) | copy-start | bytes 3145732
  44.5 65.8 %all-gather.4.cloned.1.call-start = ((), (), s32[]{:S(2)}) async-start(), calls=%async_computation.5 | async-start | bytes 3932160 | tf_op jit(solution)/shard_map/all_gather | solution.py:107
  82.6 4.0 %copy-start.4 = (bf16[1,2048,256]{2,1,0:T(8,128)(2,1)S(1)}, bf16[1,2048,256]{2,1,0:T(8,128)(2,1)}, u32[]{:S(2)}) copy-start(bf16[1,2048,256]{2,1,0:T(8,128)(2,1)} %param.24) | copy-start | bytes 3145732
  82.6 73.1 %reduce-scatter.3.cloned.1.call-start = ((), (), s32[]{:S(2)}) async-start(), calls=%async_computation.7 | async-start | bytes 3932160 | tf_op jit(solution)/shard_map/reduce_scatter | solution.py:123
  82.7 3.9 %copy-start.10 = (bf16[768,2048]{1,0:T(8,128)(2,1)S(1)}, bf16[768,2048]{1,0:T(8,128)(2,1)}, u32[]{:S(2)}) copy-start(bf16[768,2048]{1,0:T(8,128)(2,1)} %all-gather.6.cloned.1.call-done) | copy-start | bytes 9437188
  155.8 25.6 %all-to-all-start.2 = ((bf16[8,96,512]{2,1,0:T(8,128)(2,1)}), bf16[8,96,512]{2,1,0:T(8,128)(2,1)S(1)}, u32[]{:S(2)}, u32[]{:S(2)}) async-start(bf16[8,96,512]{2,1,0:T(8,128)(2,1)} %bitcast.89), calls=%async_computation.3 | async-start | bytes 1572864 | tf_op jit(solution)/shard_map/all_to_all | solution.py:132
  161.3 40.6 %all-gather.8.cloned.1.call-start = ((), (), s32[]{:S(2)}) async-start(), calls=%async_computation.8 | async-start | bytes 1310720 | tf_op jit(solution)/shard_map/all_gather | solution.py:136
  183.3 3.7 %copy-start.2 = (bf16[256,256]{1,0:T(8,128)(2,1)S(1)}, bf16[256,256]{1,0:T(8,128)(2,1)}, u32[]{:S(2)}) copy-start(bf16[256,256]{1,0:T(8,128)(2,1)} %param.15) | copy-start | bytes 393220
  183.3 18.5 %copy-start.9 = (f32[256]{0:T(256)S(1)}, f32[256]{0:T(256)}, u32[]{:S(2)}) copy-start(f32[256]{0:T(256)} %param.17) | copy-start | bytes 3076
  187.0 18.1 %copy-start.7 = (f32[31,256]{1,0:T(8,128)S(1)}, f32[31,256]{1,0:T(8,128)}, u32[]{:S(2)}) copy-start(f32[31,256]{1,0:T(8,128)} %param.16) | copy-start | bytes 95236
  187.0 87.0 %reduce-scatter.5.cloned.1.call-start = ((), (), s32[]{:S(2)}) async-start(), calls=%async_computation.9 | async-start | bytes 2359296 | tf_op jit(solution)/shard_map/reduce_scatter | solution.py:151
  205.1 4.1 %copy-start.11 = (bf16[768,2048]{1,0:T(8,128)(2,1)S(1)}, bf16[768,2048]{1,0:T(8,128)(2,1)}, u32[]{:S(2)}) copy-start(bf16[768,2048]{1,0:T(8,128)(2,1)} %all-gather.4.cloned.1.call-done) | copy-start | bytes 9437188
  205.1 4.1 %copy-start.13 = (f32[768,256]{1,0:T(8,128)S(1)}, f32[768,256]{1,0:T(8,128)}, u32[]{:S(2)}) copy-start(f32[768,256]{1,0:T(8,128)} %fusion.9) | copy-start | bytes 2359300
  205.1 4.1 %copy-start.14 = (f32[768,256]{1,0:T(8,128)S(1)}, f32[768,256]{1,0:T(8,128)}, u32[]{:S(2)}) copy-start(f32[768,256]{1,0:T(8,128)} %fusion.12) | copy-start | bytes 2359300
  209.2 2.1 copy-start.3
  209.2 2.0 copy-start.12
  218.4 8.9 %collective-permute-start = (bf16[15,256]{1,0:T(8,128)(2,1)S(1)}, bf16[15,256]{1,0:T(8,128)(2,1)S(1)}, u32[]{:S(2)}, u32[]{:S(2)}) collective-permute-start(bf16[15,256]{1,0:T(8,128)(2,1)S(1)} %get-tuple-element.18), channel_id=1, source_target_pairs={{0,4},{4,8},{8,12},{12,16},{16,20},{20,24},{24,28},{1,5},{5,9},{9,... | collective-permute-start | bytes 23048 | tf_op jit(solution)/shard_map/ppermute | solution.py:16
  221.9 5.8 %copy-start.5 = (bf16[256,256]{1,0:T(8,128)(2,1)S(1)}, bf16[256,256]{1,0:T(8,128)(2,1)}, u32[]{:S(2)}) copy-start(bf16[256,256]{1,0:T(8,128)(2,1)} %param.14) | copy-start | bytes 393220
  221.9 5.8 %copy-start.6 = (bf16[256,256]{1,0:T(8,128)(2,1)S(1)}, bf16[256,256]{1,0:T(8,128)(2,1)}, u32[]{:S(2)}) copy-start(bf16[256,256]{1,0:T(8,128)(2,1)} %param.13) | copy-start | bytes 393220
  221.9 5.7 %collective-permute-start.1 = (bf16[15,256]{1,0:T(8,128)(2,1)S(1)}, bf16[15,256]{1,0:T(8,128)(2,1)S(1)}, u32[]{:S(2)}, u32[]{:S(2)}) collective-permute-start(bf16[15,256]{1,0:T(8,128)(2,1)S(1)} %get-tuple-element.19), channel_id=1, source_target_pairs={{4,0},{8,4},{12,8},{16,12},{20,16},{24,20},{28,24},{5,1},{9,5},{13... | collective-permute-start | bytes 23048 | tf_op jit(solution)/shard_map/ppermute | solution.py:17
Sparse Core Ops, SparseCore 0:
  44.6 27.5 all-gather.5
  82.7 27.5 all-gather.3
  118.0 37.7 reduce-scatter.2
  187.1 14.6 all-gather.7
  205.8 68.1 reduce-scatter.4
where the time goes:
time: 281 us
  waiting for transfers between devices  133 us (47%)
  blocking collectives  62.7 us (22%)
  matrix products  27.1 us (10%)
  local copies, waits for them, and re-layouts  23.9 us (9%)
  between operations  14.2 us (5%)
  starting transfers between devices  10.8 us (4%)
  other arithmetic  9.13 us (3%)
    reduce_scatter x1, waiting for transfers between devices, per_device(): lax.psum_scatter(lax.dot_general(grad_mix, heads, (((0,), (0,)), ((), ())...  44 us
    reduce_scatter x1, waiting for transfers between devices, per_device(): lax.psum_scatter(partial_value, 'tp', scatter_dimension=2, tiled=True)  37.9 us
    all_to_all x1, blocking collectives, per_device(): lax.all_to_all(in_pad[token_idx], 'sp', split_axis=0, concat_axis=0, tile...  27.3 us
    all_to_all x1, blocking collectives, per_device(): lax.all_to_all(cot_pad[owner_idx], 'sp', split_axis=0, concat_axis=0, til...  23.1 us
    all_gather x1, waiting for transfers between devices, per_device(): lax.all_gather(sent_cot, 'tp', axis=1, tiled=True)  21.8 us
    all_to_all x1, waiting for transfers between devices, per_device(): lax.all_to_all(row_grads, 'sp', split_axis=0, concat_axis=0, tiled=True)  19.8 us
    mul x3, local copies, waits for them, and re-layouts, per_device(): grad_out.astype(jnp.float32)[:, None, :] * route_weights[:, :, None]  10.6 us
    all_gather x1, waiting for transfers between devices, per_device(): grad_mix = lax.all_gather(mix_part, 'tp', axis=1, tiled=True)  8.7 us
  transfers between devices with their start and end apart: 8, of which 6 were waited for; matrix products, arithmetic and copies ran while one was open for 12% of the time, Pallas kernels for 0%

commit v1 on v0

--- a/solution.py
+++ b/solution.py
@@ -104,7 +104,9 @@
     )
     recv_in, recv_cot = (
         lax.all_gather(sent_in, "tp", axis=1, tiled=True),
-        lax.all_gather(sent_cot, "tp", axis=1, tiled=True),
+        jnp.concatenate(
+            lax.all_to_all(jnp.stack([sent_cot] * lax.axis_size("tp")), "tp", 0, 0), axis=1
+        ),
     )
     in_rows = to_expert(recv_in)
     cot_rows = to_expert(recv_cot)

time: 281 us -> 295 us (1.050)
  waiting for transfers between devices: 133 us -> 138 us
  starting transfers between devices: 10.8 us -> 15.5 us
    all_to_all x0 -> x1, waiting for transfers between devices: none -> 31.1 us  [per_device(): lax.all_to_all(jnp.stack([sent_cot] * lax.axis_size('tp')), 'tp', 0, 0)]
    all_gather x1 -> x0, waiting for transfers between devices: 21.8 us -> none  [per_device(): lax.all_gather(sent_cot, 'tp', axis=1, tiled=True)]
    all_to_all x0 -> x1, starting transfers between devices: none -> 4.65 us  [per_device(): lax.all_to_all(jnp.stack([sent_cot] * lax.axis_size('tp')), 'tp', 0, 0)]
  transfers between devices with their start and end apart: 8 -> 8, of which waited for: 6 -> 6; matrix products, arithmetic and copies ran while one was open for 12% -> 13% of each run, Pallas kernels for 0% -> 0%
where the time goes in v1:
time: 295 us
  waiting for transfers between devices  138 us (47%)
  blocking collectives  62.6 us (21%)
  matrix products  29.1 us (10%)
  local copies, waits for them, and re-layouts  26.1 us (9%)
  starting transfers between devices  15.5 us (5%)
  between operations  14.2 us (5%)
  other arithmetic  9.13 us (3%)
    reduce_scatter x1, waiting for transfers between devices, per_device(): lax.psum_scatter(lax.dot_general(grad_mix, heads, (((0,), (0,)), ((), ())...  42.1 us
    reduce_scatter x1, waiting for transfers between devices, per_device(): lax.psum_scatter(partial_value, 'tp', scatter_dimension=2, tiled=True)  35.9 us
    all_to_all x1, waiting for transfers between devices, per_device(): lax.all_to_all(jnp.stack([sent_cot] * lax.axis_size('tp')), 'tp', 0, 0)  31.1 us
    all_to_all x1, blocking collectives, per_device(): lax.all_to_all(in_pad[token_idx], 'sp', split_axis=0, concat_axis=0, tile...  27.3 us
    all_to_all x1, blocking collectives, per_device(): lax.all_to_all(cot_pad[owner_idx], 'sp', split_axis=0, concat_axis=0, til...  23 us
    all_to_all x1, waiting for transfers between devices, per_device(): lax.all_to_all(row_grads, 'sp', split_axis=0, concat_axis=0, tiled=True)  19.8 us
    mul x3, local copies, waits for them, and re-layouts, per_device(): grad_out.astype(jnp.float32)[:, None, :] * route_weights[:, :, None]  10.7 us
    all_gather x1, waiting for transfers between devices, per_device(): grad_mix = lax.all_gather(mix_part, 'tp', axis=1, tiled=True)  8.67 us
  transfers between devices with their start and end apart: 8, of which 6 were waited for; matrix products, arithmetic and copies ran while one was open for 13% of the time, Pallas kernels for 0%

profile of v1, /device:TPU:0, one launch (start us, length us, event | category | flops | bytes accessed | tf_op | source)
XLA Modules:
  0.0 294.6 jit_solution(11963395521060101775)
XLA Ops:
  10.9 2.4 scatter_custom_fusion
  14.4 2.7 gather_fusion.1
  17.1 27.3 %all_to_all.38 = bf16[8,96,512]{2,1,0:T(8,128)(2,1)} all-to-all(bf16[8,96,512]{2,1,0:T(8,128)(2,1)S(1)} %bitcast.88), channel_id=1, replica_groups=mesh['sp'=8,'tp'=4] {'sp'}, dimensions={0} | all-to-all | bytes 1572864 | tf_op jit(solution)/shard_map/all_to_all | solution.py:102
  44.8 4.1 %mul.456 = f32[256,2,2048]{2,1,0:T(2,128)} broadcast(bf16[256,2048]{1,0:T(8,128)(2,1)S(1)} %copy-done.1), dimensions={0,2} | broadcast | bytes 5242880 | tf_op jit(solution)/shard_map/mul | solution.py:84
  48.9 6.4 %mul.457 = f32[512,2048]{1,0:T(8,128)} reshape(f32[256,2,2048]{2,1,0:T(2,128)} %mul.456) | data formatting | bytes 8388608 | tf_op jit(solution)/shard_map/mul | solution.py:84
  55.3 1.4 fusion.6
  56.7 2.7 gather_fusion
  59.4 23.0 %all_to_all.39 = bf16[8,96,512]{2,1,0:T(8,128)(2,1)S(1)} all-to-all(bf16[8,96,512]{2,1,0:T(8,128)(2,1)S(1)} %bitcast.89), channel_id=1, replica_groups=mesh['sp'=8,'tp'=4] {'sp'}, dimensions={0} | all-to-all | bytes 1572864 | tf_op jit(solution)/shard_map/all_to_all | solution.py:103
  82.7 1.9 stack.10
  84.6 4.6 %all-to-all-start.1 = ((bf16[4,768,512]{1,2,0:T(8,128)(2,1)}), bf16[4,768,512]{1,2,0:T(8,128)(2,1)}, u32[]{:S(2)}, u32[]{:S(2)}) async-start(bf16[4,768,512]{1,2,0:T(8,128)(2,1)} %stack.10), calls=%async_computation.1 | async-start | bytes 6291456 | tf_op jit(solution)/shard_map/all_to_all | solution.py:108
  89.4 3.9 %fusion.9 = f32[768,256]{1,0:T(8,128)} fusion(bf16[768,2048]{1,0:T(8,128)(2,1)} %all-gather.3.cloned.1.call-done, bf16[1,2048,256]{2,1,0:T(8,128)(2,1)S(1)} %copy-done), kind=kOutput, calls=%fused_computation.19 | convolution fusion | flops 805306368 | bytes 4980736 | tf_op jit(solution)/shard_map/esd,edf->esf/dot_general | solution.py:23
  93.3 1.9 fusion.12
  95.1 31.1 %all-to-all-done.1 = bf16[4,768,512]{1,2,0:T(8,128)(2,1)} async-done(((bf16[4,768,512]{1,2,0:T(8,128)(2,1)}), bf16[4,768,512]{1,2,0:T(8,128)(2,1)}, u32[]{:S(2)}, u32[]{:S(2)}) %all-to-all-start.1) | async-done | bytes 3145760 | tf_op jit(solution)/shard_map/all_to_all | solution.py:108
  126.2 3.8 %multiply_convert_fusion.1 = (bf16[768,256]{1,0:T(8,128)(2,1)S(1)}, bf16[768,256]{1,0:T(8,128)(2,1)S(1)}) fusion(f32[768,256]{1,0:T(8,128)} %fusion.9, f32[768,256]{1,0:T(8,128)} %fusion.12, bf16[768,2048]{0,1:T(8,128)(2,1)} %bitcast.8, bf16[1,256,2048]{2,1,0:T(8,128)(2,1)} %param.25), kind=kOutput, calls=%fused_computation.27 | convolution fusion | flops 807862272 | bytes 6553600 | tf_op jit(solution)/shard_map/esd,efd->esf/dot_general | solution.py:28
  131.0 2.7 fusion
  133.8 35.9 %reduce-scatter.3.cloned.1.call-done = bf16[1,768,512]{2,1,0:T(8,128)(2,1)} async-done(((bf16[1,768,2048]{2,1,0:T(8,128)(2,1)}), bf16[1,768,512]{2,1,0:T(8,128)(2,1)}) %reduce-scatter.3.cloned.1.call-update) | async-done | bytes 786448 | tf_op jit(solution)/shard_map/reduce_scatter | solution.py:125
  169.7 5.5 %all-to-all-start.3 = ((bf16[8,96,512]{2,1,0:T(8,128)(2,1)}), bf16[8,96,512]{2,1,0:T(8,128)(2,1)S(1)}, u32[]{:S(2)}, u32[]{:S(2)}) async-start(bf16[8,96,512]{2,1,0:T(8,128)(2,1)} %bitcast.92), calls=%async_computation.4 | async-start | bytes 1572864 | tf_op jit(solution)/shard_map/all_to_all | solution.py:134
  175.5 19.8 %all-to-all-done.3 = bf16[8,96,512]{2,1,0:T(8,128)(2,1)S(1)} async-done(((bf16[8,96,512]{2,1,0:T(8,128)(2,1)}), bf16[8,96,512]{2,1,0:T(8,128)(2,1)S(1)}, u32[]{:S(2)}, u32[]{:S(2)}) %all-to-all-start.3) | async-done | bytes 786464 | tf_op jit(solution)/shard_map/all_to_all | solution.py:134
  195.3 2.0 gather_fusion.2
  198.0 1.2 reduce_sum.60
  199.2 1.7 add_convert_fusion.1
  201.2 5.9 %all-reduce.3 = (f32[256]{0:T(256)S(1)}, f32[256]{0:T(256)S(1)}) all-reduce(f32[256]{0:T(256)S(1)} %get-tuple-element.9, f32[256]{0:T(256)S(1)} %get-tuple-element.8), channel_id=1, replica_groups=mesh['sp'=8,'tp'=4] {'tp'}, use_global_device_ids=true, to_apply=%region_3.4 | all-reduce | flops 512 | bytes 4096 | tf_op jit(solution)/shard_map/psum | solution.py:143
  207.1 8.7 %all-gather.5.cloned.1.call-done = bf16[256,2048]{1,0:T(8,128)(2,1)} async-done(((bf16[256,512]{1,0:T(8,128)(2,1)}), bf16[256,2048]{1,0:T(8,128)(2,1)}) %all-gather.5.cloned.1.call-update) | async-done | bytes 1048592 | tf_op jit(solution)/shard_map/all_gather | solution.py:138
  215.8 3.2 %fusion.65 = f32[2048,256]{1,0:T(8,128)} fusion(bf16[256,2048]{1,0:T(8,128)(2,1)} %all-gather.5.cloned.1.call-done, bf16[256,256]{1,0:T(8,128)(2,1)S(1)} %copy-done.2, f32[256]{0:T(256)S(1)} %copy-done.9, f32[256]{0:T(256)S(1)} %get-tuple-element.54, f32[256]{0:T(256)S(1)} %get-tuple-element.53), kind=kOutput, calls=%fused_computation.117 | convolution fusion | flops 269025280 | bytes 3279872 | tf_op jit(solution)/shard_map/dot_general | solution.py:154
  219.1 4.0 %fusion.2 = bf16[1,2048,256]{2,1,0:T(8,128)(2,1)} fusion(bf16[768,2048]{1,0:T(8,128)(2,1)} %all-gather.3.cloned.1.call-done, bf16[768,256]{1,0:T(8,128)(2,1)S(1)} %get-tuple-element.16), kind=kOutput, calls=%fused_computation.10 | convolution fusion | flops 805830656 | bytes 4587520 | tf_op jit(solution)/shard_map/esd,esf->edf/dot_general | solution.py:43
  223.1 4.1 %fusion.3 = bf16[1,256,2048]{2,1,0:T(8,128)(2,1)} fusion(bf16[768,2048]{0,1:T(8,128)(2,1)} %bitcast.8, f32[768,256]{1,0:T(8,128)S(1)} %copy-done.13, f32[768,256]{1,0:T(8,128)S(1)} %copy-done.12), kind=kOutput, calls=%fused_computation.11 | convolution fusion | flops 807010304 | bytes 5767168 | tf_op jit(solution)/shard_map/esf,esd->efd/dot_general | solution.py:37
  227.8 6.3 %all-reduce.2 = (f32[256]{0:T(256)S(1)}, f32[256]{0:T(256)S(1)}) all-reduce(f32[256]{0:T(256)S(1)} %get-tuple-element.7, f32[256]{0:T(256)S(1)} %get-tuple-element.6), channel_id=1, replica_groups=mesh['sp'=8,'tp'=4] {'tp'}, use_global_device_ids=true, to_apply=%region_13.14 | all-reduce | flops 512 | bytes 4096 | tf_op jit(solution)/shard_map/psum | solution.py:167
  234.3 3.5 %collective-permute-start = (bf16[15,256]{1,0:T(8,128)(2,1)S(1)}, bf16[15,256]{1,0:T(8,128)(2,1)S(1)}, u32[]{:S(2)}, u32[]{:S(2)}) collective-permute-start(bf16[15,256]{1,0:T(8,128)(2,1)S(1)} %get-tuple-element.18), channel_id=1, source_target_pairs={{0,4},{4,8},{8,12},{12,16},{16,20},{20,24},{24,28},{1,5},{5,9},{9,... | collective-permute-start | bytes 23048 | tf_op jit(solution)/shard_map/ppermute | solution.py:16
  237.9 1.4 collective-permute-start.1
  239.3 4.0 %fusion.1 = bf16[1,2048,256]{2,1,0:T(8,128)(2,1)} fusion(bf16[768,2048]{1,0:T(8,128)(2,1)} %all-gather.3.cloned.1.call-done, bf16[768,256]{1,0:T(8,128)(2,1)S(1)} %get-tuple-element.17), kind=kOutput, calls=%fused_computation.9 | convolution fusion | flops 805830656 | bytes 4587520 | tf_op jit(solution)/shard_map/esd,esf->edf/dot_general | solution.py:40
  243.6 1.6 multiply_convert_fusion.4
  245.9 42.1 %reduce-scatter.5.cloned.1.call-done = f32[256,256]{1,0:T(8,128)} async-done(((f32[2048,256]{1,0:T(8,128)}), f32[256,256]{1,0:T(8,128)}) %reduce-scatter.5.cloned.1.call-update) | async-done | bytes 262160 | tf_op jit(solution)/shard_map/reduce_scatter | solution.py:153
  (75 shorter events, 9.5 us)
Async XLA Ops:
  7.2 82.2 %copy-start = (bf16[1,2048,256]{2,1,0:T(8,128)(2,1)S(1)}, bf16[1,2048,256]{2,1,0:T(8,128)(2,1)}, u32[]{:S(2)}) copy-start(bf16[1,2048,256]{2,1,0:T(8,128)(2,1)} %param.23) | copy-start | bytes 3145732
  7.2 82.2 %all-gather.3.cloned.1.call-start = ((), (), s32[]{:S(2)}) async-start(), calls=%async_computation.6 | async-start | bytes 3932160 | tf_op jit(solution)/shard_map/all_gather | solution.py:106
  14.4 30.1 %copy-start.8 = (f32[256,2]{0,1:T(2,128)S(1)}, f32[256,2]{0,1:T(2,128)}, u32[]{:S(2)}) copy-start(f32[256,2]{0,1:T(2,128)} %param.22) | copy-start | bytes 6148
  14.4 30.4 %copy-start.1 = (bf16[256,2048]{1,0:T(8,128)(2,1)S(1)}, bf16[256,2048]{1,0:T(8,128)(2,1)}, u32[]{:S(2)}) copy-start(bf16[256,2048]{1,0:T(8,128)(2,1)} %param.20) | copy-start | bytes 3145732
  84.6 41.6 %all-to-all-start.1 = ((bf16[4,768,512]{1,2,0:T(8,128)(2,1)}), bf16[4,768,512]{1,2,0:T(8,128)(2,1)}, u32[]{:S(2)}, u32[]{:S(2)}) async-start(bf16[4,768,512]{1,2,0:T(8,128)(2,1)} %stack.10), calls=%async_computation.1 | async-start | bytes 6291456 | tf_op jit(solution)/shard_map/all_to_all | solution.py:108
  89.3 4.0 %copy-start.4 = (bf16[1,2048,256]{2,1,0:T(8,128)(2,1)S(1)}, bf16[1,2048,256]{2,1,0:T(8,128)(2,1)}, u32[]{:S(2)}) copy-start(bf16[1,2048,256]{2,1,0:T(8,128)(2,1)} %param.24) | copy-start | bytes 3145732
  89.3 80.5 %reduce-scatter.3.cloned.1.call-start = ((), (), s32[]{:S(2)}) async-start(), calls=%async_computation.7 | async-start | bytes 3932160 | tf_op jit(solution)/shard_map/reduce_scatter | solution.py:125
  89.3 3.9 %copy-start.10 = (bf16[768,2048]{1,0:T(8,128)(2,1)S(1)}, bf16[768,2048]{1,0:T(8,128)(2,1)}, u32[]{:S(2)}) copy-start(bf16[768,2048]{1,0:T(8,128)(2,1)} %all-gather.3.cloned.1.call-done) | copy-start | bytes 9437188
  169.7 25.6 %all-to-all-start.3 = ((bf16[8,96,512]{2,1,0:T(8,128)(2,1)}), bf16[8,96,512]{2,1,0:T(8,128)(2,1)S(1)}, u32[]{:S(2)}, u32[]{:S(2)}) async-start(bf16[8,96,512]{2,1,0:T(8,128)(2,1)} %bitcast.92), calls=%async_computation.4 | async-start | bytes 1572864 | tf_op jit(solution)/shard_map/all_to_all | solution.py:134
  175.2 40.6 %all-gather.5.cloned.1.call-start = ((), (), s32[]{:S(2)}) async-start(), calls=%async_computation.8 | async-start | bytes 1310720 | tf_op jit(solution)/shard_map/all_gather | solution.py:138
  197.3 3.7 %copy-start.2 = (bf16[256,256]{1,0:T(8,128)(2,1)S(1)}, bf16[256,256]{1,0:T(8,128)(2,1)}, u32[]{:S(2)}) copy-start(bf16[256,256]{1,0:T(8,128)(2,1)} %param.15) | copy-start | bytes 393220
  197.3 18.5 %copy-start.9 = (f32[256]{0:T(256)S(1)}, f32[256]{0:T(256)}, u32[]{:S(2)}) copy-start(f32[256]{0:T(256)} %param.17) | copy-start | bytes 3076
  200.9 18.1 %copy-start.7 = (f32[31,256]{1,0:T(8,128)S(1)}, f32[31,256]{1,0:T(8,128)}, u32[]{:S(2)}) copy-start(f32[31,256]{1,0:T(8,128)} %param.16) | copy-start | bytes 95236
  201.0 87.1 %reduce-scatter.5.cloned.1.call-start = ((), (), s32[]{:S(2)}) async-start(), calls=%async_computation.9 | async-start | bytes 2359296 | tf_op jit(solution)/shard_map/reduce_scatter | solution.py:153
  219.1 4.0 %copy-start.12 = (f32[768,256]{1,0:T(8,128)S(1)}, f32[768,256]{1,0:T(8,128)}, u32[]{:S(2)}) copy-start(f32[768,256]{1,0:T(8,128)} %fusion.9) | copy-start | bytes 2359300
  219.1 4.0 %copy-start.13 = (f32[768,256]{1,0:T(8,128)S(1)}, f32[768,256]{1,0:T(8,128)}, u32[]{:S(2)}) copy-start(f32[768,256]{1,0:T(8,128)} %fusion.12) | copy-start | bytes 2359300
  223.1 4.1 %copy-start.3 = (bf16[256,2048]{1,0:T(8,128)(2,1)S(1)}, bf16[256,2048]{1,0:T(8,128)(2,1)}, u32[]{:S(2)}) copy-start(bf16[256,2048]{1,0:T(8,128)(2,1)} %all-gather.5.cloned.1.call-done) | copy-start | bytes 3145732
  223.1 4.1 %copy-start.11 = (bf16[256,2048]{1,0:T(8,128)(2,1)S(1)}, bf16[256,2048]{1,0:T(8,128)(2,1)}, u32[]{:S(2)}) copy-start(bf16[256,2048]{1,0:T(8,128)(2,1)} %param.18) | copy-start | bytes 3145732
  234.3 9.0 %collective-permute-start = (bf16[15,256]{1,0:T(8,128)(2,1)S(1)}, bf16[15,256]{1,0:T(8,128)(2,1)S(1)}, u32[]{:S(2)}, u32[]{:S(2)}) collective-permute-start(bf16[15,256]{1,0:T(8,128)(2,1)S(1)} %get-tuple-element.18), channel_id=1, source_target_pairs={{0,4},{4,8},{8,12},{12,16},{16,20},{20,24},{24,28},{1,5},{5,9},{9,... | collective-permute-start | bytes 23048 | tf_op jit(solution)/shard_map/ppermute | solution.py:16
  237.8 5.7 %copy-start.5 = (bf16[256,256]{1,0:T(8,128)(2,1)S(1)}, bf16[256,256]{1,0:T(8,128)(2,1)}, u32[]{:S(2)}) copy-start(bf16[256,256]{1,0:T(8,128)(2,1)} %param.14) | copy-start | bytes 393220
  237.9 5.7 %copy-start.6 = (bf16[256,256]{1,0:T(8,128)(2,1)S(1)}, bf16[256,256]{1,0:T(8,128)(2,1)}, u32[]{:S(2)}) copy-start(bf16[256,256]{1,0:T(8,128)(2,1)} %param.13) | copy-start | bytes 393220
  237.9 5.7 %collective-permute-start.1 = (bf16[15,256]{1,0:T(8,128)(2,1)S(1)}, bf16[15,256]{1,0:T(8,128)(2,1)S(1)}, u32[]{:S(2)}, u32[]{:S(2)}) collective-permute-start(bf16[15,256]{1,0:T(8,128)(2,1)S(1)} %get-tuple-element.19), channel_id=1, source_target_pairs={{4,0},{8,4},{12,8},{16,12},{20,16},{24,20},{28,24},{5,1},{9,5},{13... | collective-permute-start | bytes 23048 | tf_op jit(solution)/shard_map/ppermute | solution.py:17
Sparse Core Ops, SparseCore 0:
  44.6 27.5 all-gather.2
  133.9 35.7 reduce-scatter.2
  201.1 14.6 all-gather.4
  219.8 68.2 reduce-scatter.4
